TPU v7x, 32 devices: a whole 2x2x4 slice. The times are simulated.
32 devices in a mesh: rep: 2 (over y), fs: 4 (over z), tp: 4 (over x, core).
Axes of the slice: x: 2, y: 2, z: 4, core: 2. Of those that a mesh axis runs over, the one named last changes fastest.
Arguments:
- out_grad: bfloat16 [2048, 2048], P(('rep', 'fs'), 'tp'), may hold values from -6 to 6
- gate_lin: bfloat16 [2048, 5632], P(('rep', 'fs'), 'tp'), may hold values from -6 to 6
- up_lin: bfloat16 [2048, 5632], P(('rep', 'fs'), 'tp'), may hold values from -6 to 6
- conv_weight: bfloat16 [3, 5632], replicated, may hold values from -3.5 to 3.5
- gate_weight: bfloat16 [2048, 5632], P('fs', 'tp'), may hold values from -0.125 to 0.125
- up_weight: bfloat16 [2048, 5632], P('fs', 'tp'), may hold values from -0.125 to 0.125
- down_weight: bfloat16 [5632, 2048], P('tp', 'fs'), may hold values from -0.078125 to 0.078125
Outputs:
- input_grad: bfloat16 [2048, 2048], P(('rep', 'fs'), 'tp')
- conv_grad: float32 [3, 5632], replicated
All inputs are finite; a program needn't handle non-finite values.
Results may differ from a plain program's by a relative error of at most 0.015.
Values may be sent and summed in bfloat16 or wider, within the bound.
A program may use at most 64 MiB of HBM per device.

v0:
```python
import math
import jax
import jax.numpy as jnp
from jax import lax
from jax.sharding import PartitionSpec as P


def extended(value, sides, width):
    for axis, dim in sides:
        peers, length = (lax.axis_size(axis), value.shape[dim])
        up = [(i, (i + 1) % peers) for i in range(peers - 1)]
        down = [(j, i) for i, j in up]
        last = lax.slice_in_dim(value, length - width, length, axis=dim)
        leading = lax.slice_in_dim(value, 0, width, axis=dim)
        before = lax.ppermute(last, axis, up)
        after = lax.ppermute(leading, axis, down)
        value = jnp.concatenate([before, value, after], axis=dim)
    return value


def gelu_parts(gate):
    normal_cdf = 0.5 * (1.0 + jax.scipy.special.erf(gate * (1.0 / math.sqrt(2.0))))
    density = jnp.exp(-0.5 * gate * gate) * (1.0 / math.sqrt(2.0 * math.pi))
    return (gate * normal_cdf, normal_cdf + gate * density)


def local(out_grad, gate_lin, up_lin, conv_weight, gate_weight, up_weight, down_weight):
    conv_full = conv_weight.astype(jnp.float32)
    column_count = gate_lin.shape[1]
    column_start = lax.axis_index("tp") * column_count
    conv_taps = lax.dynamic_slice_in_dim(conv_full, column_start, column_count, 1)
    grad_rows = lax.all_gather(out_grad, "tp", axis=1, tiled=True)
    act_grad = lax.dot_general(
        grad_rows,
        lax.all_gather(down_weight, "fs", axis=1, tiled=True),
        (((1,), (1,)), ((), ())),
        preferred_element_type=jnp.float32,
    )
    linear_mid = extended(gate_lin, (("fs", 0),), 1).astype(jnp.float32)
    gate = (
        conv_taps[0] * linear_mid[:-2]
        + conv_taps[1] * linear_mid[1:-1]
        + conv_taps[2] * linear_mid[2:]
    )
    gelu_value, gelu_slope = gelu_parts(gate)
    gate_grad = act_grad * up_lin.astype(jnp.float32) * gelu_slope
    grad_ext = extended(gate_grad.astype(jnp.bfloat16), (("fs", 0),), 1).astype(gate_grad.dtype)
    up_grad = (act_grad * gelu_value).astype(jnp.bfloat16)
    own_grad = grad_ext[1:-1]
    linear_grad = (
        conv_taps[0] * grad_ext[2:] + conv_taps[1] * own_grad + conv_taps[2] * grad_ext[:-2]
    ).astype(jnp.bfloat16)
    local_conv = jnp.stack(
        [
            jnp.sum(own_grad * linear_mid[:-2], axis=0),
            jnp.sum(own_grad * linear_mid[1:-1], axis=0),
            jnp.sum(own_grad * linear_mid[2:], axis=0),
        ]
    )
    product = lax.dot_general(
        linear_grad,
        lax.all_gather(gate_weight, "fs", axis=0, tiled=True),
        (((1,), (1,)), ((), ())),
        preferred_element_type=jnp.float32,
    )
    product = product + lax.dot_general(
        up_grad,
        lax.all_gather(up_weight, "fs", axis=0, tiled=True),
        (((1,), (1,)), ((), ())),
        preferred_element_type=jnp.float32,
    )
    input_grad = lax.psum_scatter(
        product.astype(jnp.bfloat16), "tp", scatter_dimension=1, tiled=True
    )
    summed_conv = lax.psum(local_conv, ("rep", "fs"))
    conv_grad = lax.all_gather(summed_conv, "tp", axis=1, tiled=True)
    return (input_grad, conv_grad)


def solution(mesh):
    return jax.shard_map(
        local,
        mesh=mesh,
        in_specs=(
            P(("rep", "fs"), "tp"),
            P(("rep", "fs"), "tp"),
            P(("rep", "fs"), "tp"),
            P(),
            P("fs", "tp"),
            P("fs", "tp"),
            P("tp", "fs"),
        ),
        out_specs=(P(("rep", "fs"), "tp"), P()),
        check_vma=False,
    )
```

profile of v0, /device:TPU:0, one launch (start us, length us, event | category | flops | bytes accessed | tf_op | source)
XLA Modules:
  0.0 404.9 jit_solution(1864692760127615159)
XLA Ops:
  7.2 0.0 all-gather.5.cloned.1.call-start
  7.2 0.7 all-gather.5.cloned.1.call-update
  7.9 0.0 all-gather.7.cloned.1.call-start
  7.9 0.7 all-gather.7.cloned.1.call-update
  8.6 0.0 copy-start
  8.7 0.0 all-gather.9.cloned.1.call-start
  8.7 0.7 all-gather.9.cloned.1.call-update
  9.4 0.0 all-gather.11.cloned.1.call-start
  9.4 0.5 all-gather.11.cloned.1.call-update
  10.0 0.0 copy-start.1
  10.0 0.0 reduce-scatter.2.cloned.1.call-start
  10.0 0.0 copy-done
  10.1 5.1 %collective-permute-start = (bf16[1,1408]{1,0:T(2,128)(2,1)S(1)}, bf16[1,1408]{1,0:T(2,128)(2,1)S(1)}, u32[]{:S(2)}, u32[]{:S(2)}) collective-permute-start(bf16[1,1408]{1,0:T(2,128)(2,1)S(1)} %get-tuple-element.12), channel_id=1, source_target_pairs={{0,4},{4,8},{8,12},{1,5},{5,9},{9,13},{2,6},{6,10},{10,14},{3,7},{... | collective-permute-start | bytes 8456 | tf_op jit(solution)/shard_map/ppermute | solution.py:15
  15.2 1.3 collective-permute-start.1
  16.5 0.7 dynamic-slice_convert_fusion
  17.2 0.1 slice_reduce_fusion.2
  17.2 0.0 collective-permute-done
  17.2 3.4 collective-permute-done.1
  20.7 0.2 maximum_convert_fusion
  20.8 8.2 %all-gather.5.cloned.1.call-done = bf16[256,2048]{1,0:T(8,128)(2,1)} async-done(((bf16[256,512]{1,0:T(8,128)(2,1)}), bf16[256,2048]{1,0:T(8,128)(2,1)}) %all-gather.5.cloned.1.call-update) | async-done | bytes 1048592 | tf_op jit(solution)/shard_map/all_gather | solution.py:32
  29.0 108.3 %all-gather.7.cloned.1.call-done = bf16[1408,2048]{1,0:T(8,128)(2,1)} async-done(((bf16[1408,512]{1,0:T(8,128)(2,1)}), bf16[1408,2048]{1,0:T(8,128)(2,1)}) %all-gather.7.cloned.1.call-update) | async-done | bytes 5767184 | tf_op jit(solution)/shard_map/all_gather | solution.py:35
  137.3 0.0 copy-done.1
  137.3 7.2 %fusion.6 = (bf16[256,1408]{1,0:T(8,128)(2,1)S(1)}, f32[256,1408]{1,0:T(8,128)}, f32[256,1408]{1,0:T(8,128)}) fusion(bf16[256,1408]{1,0:T(8,128)(2,1)S(1)} %copy-done.1, f32[258,1408]{1,0:T(8,128)S(1)} %maximum_convert_fusion, f32[1408]{0:T(1024)S(1)} %get-tuple-element.7, f32[1408]{0:T(1024)S(1)} %get-tuple-element.6, f32[1408]{0:T(1024)S(1)} %get-tuple-element.5, ...), kind=kOutput, calls=%fused_computation.8 | convolution fusion | flops 1482522624 | bytes 15483392 | tf_op jit(solution)/shard_map/dot_general | solution.py:33
  144.5 1.3 collective-permute-start.2
  145.8 1.3 collective-permute-start.3
  147.1 0.0 collective-permute-done.2
  147.1 4.4 %collective-permute-done.3 = bf16[1,1408]{1,0:T(2,128)(2,1)S(1)} collective-permute-done((bf16[1,1408]{1,0:T(2,128)(2,1)S(1)}, bf16[1,1408]{1,0:T(2,128)(2,1)S(1)}, u32[]{:S(2)}, u32[]{:S(2)}) %collective-permute-start.3) | collective-permute-done | bytes 2848 | tf_op jit(solution)/shard_map/ppermute | solution.py:16
  151.5 0.2 maximum_convert_fusion.1
  151.7 92.3 %all-gather.9.cloned.1.call-done = bf16[2048,1408]{1,0:T(8,128)(2,1)} async-done(((bf16[512,1408]{1,0:T(8,128)(2,1)}), bf16[2048,1408]{1,0:T(8,128)(2,1)}) %all-gather.9.cloned.1.call-update) | async-done | bytes 5767184 | tf_op jit(solution)/shard_map/all_gather | solution.py:62
  244.0 6.0 %fusion.10 = f32[256,2048]{1,0:T(8,128)} fusion(bf16[2048,1408]{1,0:T(8,128)(2,1)} %all-gather.9.cloned.1.call-done, f32[258,1408]{1,0:T(8,128)S(1)} %maximum_convert_fusion.1, f32[1408]{0:T(1024)S(1)} %get-tuple-element.7, f32[1408]{0:T(1024)S(1)} %get-tuple-element.6, f32[1408]{0:T(1024)S(1)} %get-tuple-element.5), kind=kOutput, calls=%fused_computation.22 | convolution fusion | flops 1478557696 | bytes 12214272 | tf_op jit(solution)/shard_map/dot_general | solution.py:60
  249.9 100.4 %all-gather.11.cloned.1.call-done = bf16[2048,1408]{1,0:T(8,128)(2,1)} async-done(((bf16[512,1408]{1,0:T(8,128)(2,1)}), bf16[2048,1408]{1,0:T(8,128)(2,1)}) %all-gather.11.cloned.1.call-update) | async-done | bytes 5767184 | tf_op jit(solution)/shard_map/all_gather | solution.py:68
  350.3 6.9 %fusion = bf16[256,2048]{1,0:T(8,128)(2,1)} fusion(f32[256,2048]{1,0:T(8,128)} %fusion.10, bf16[2048,1408]{1,0:T(8,128)(2,1)} %all-gather.11.cloned.1.call-done, f32[256,1408]{1,0:T(8,128)} %get-tuple-element.14, f32[256,1408]{1,0:T(8,128)} %get-tuple-element.9), kind=kOutput, calls=%fused_computation.1 | convolution fusion | flops 1479606272 | bytes 11796480 | tf_op jit(solution)/shard_map/dot_general | solution.py:66
  357.2 0.0 reduce-scatter.2.cloned.1.call-update
  357.3 0.6 multiply_reduce_fusion.2
  357.9 34.5 %psum.7 = f32[3,1408]{1,0:T(4,128)S(1)} all-reduce(f32[3,1408]{1,0:T(4,128)S(1)} %pad_maximum_fusion), channel_id=1, replica_groups=mesh['rep'=2,'fs'=4,'tp'=4] {'rep','fs'}, use_global_device_ids=true, to_apply=%region_4.0 | all-reduce | flops 4224 | bytes 33792 | tf_op jit(solution)/shard_map/psum | solution.py:75
  392.4 5.3 %all_gather.19 = f32[3,5632]{1,0:T(4,128)S(1)} all-gather(f32[3,1408]{1,0:T(4,128)S(1)} %psum.7), channel_id=1, replica_groups=mesh['rep'=2,'fs'=4,'tp'=4] {'tp'}, dimensions={1}, use_global_device_ids=true | all-gather | bytes 84480 | tf_op jit(solution)/shard_map/all_gather | solution.py:76
  397.7 0.0 reduce-scatter.2.cloned.1.call-done
  397.7 0.6 copy.10
  (6 shorter events, 0.1 us)
Async XLA Ops:
  7.2 21.8 %all-gather.5.cloned.1.call-start = ((), (), s32[]{:S(2)}) async-start(), calls=%async_computation.1 | async-start | bytes 1310720 | tf_op jit(solution)/shard_map/all_gather | solution.py:32
  7.9 129.4 %all-gather.7.cloned.1.call-start = ((), (), s32[]{:S(2)}) async-start(), calls=%async_computation.2 | async-start | bytes 7208960 | tf_op jit(solution)/shard_map/all_gather | solution.py:35
  8.6 1.4 copy-start
  8.7 235.3 %all-gather.9.cloned.1.call-start = ((), (), s32[]{:S(2)}) async-start(), calls=%async_computation.3 | async-start | bytes 7208960 | tf_op jit(solution)/shard_map/all_gather | solution.py:62
  9.4 340.9 %all-gather.11.cloned.1.call-start = ((), (), s32[]{:S(2)}) async-start(), calls=%async_computation.4 | async-start | bytes 7208960 | tf_op jit(solution)/shard_map/all_gather | solution.py:68
  10.0 127.3 %copy-start.1 = (bf16[256,1408]{1,0:T(8,128)(2,1)S(1)}, bf16[256,1408]{1,0:T(8,128)(2,1)}, u32[]{:S(2)}) copy-start(bf16[256,1408]{1,0:T(8,128)(2,1)} %param.9) | copy-start | bytes 2162692
  10.0 387.7 %reduce-scatter.2.cloned.1.call-start = ((), (), s32[]{:S(2)}) async-start(), calls=%async_computation.5 | async-start | bytes 1310720 | tf_op jit(solution)/shard_map/reduce_scatter | solution.py:72
  10.1 7.2 %collective-permute-start = (bf16[1,1408]{1,0:T(2,128)(2,1)S(1)}, bf16[1,1408]{1,0:T(2,128)(2,1)S(1)}, u32[]{:S(2)}, u32[]{:S(2)}) collective-permute-start(bf16[1,1408]{1,0:T(2,128)(2,1)S(1)} %get-tuple-element.12), channel_id=1, source_target_pairs={{0,4},{4,8},{8,12},{1,5},{5,9},{9,13},{2,6},{6,10},{10,14},{3,7},{... | collective-permute-start | bytes 8456 | tf_op jit(solution)/shard_map/ppermute | solution.py:15
  15.2 5.5 %collective-permute-start.1 = (bf16[1,1408]{1,0:T(2,128)(2,1)S(1)}, bf16[1,1408]{1,0:T(2,128)(2,1)S(1)}, u32[]{:S(2)}, u32[]{:S(2)}) collective-permute-start(bf16[1,1408]{1,0:T(2,128)(2,1)S(1)} %get-tuple-element.13), channel_id=1, source_target_pairs={{4,0},{8,4},{12,8},{5,1},{9,5},{13,9},{6,2},{10,6},{14,10},{7,3},{... | collective-permute-start | bytes 8456 | tf_op jit(solution)/shard_map/ppermute | solution.py:16
  144.5 2.6 collective-permute-start.2
  145.8 5.8 %collective-permute-start.3 = (bf16[1,1408]{1,0:T(2,128)(2,1)S(1)}, bf16[1,1408]{1,0:T(2,128)(2,1)S(1)}, u32[]{:S(2)}, u32[]{:S(2)}) collective-permute-start(bf16[1,1408]{1,0:T(2,128)(2,1)S(1)} %get-tuple-element.11), channel_id=1, source_target_pairs={{4,0},{8,4},{12,8},{5,1},{9,5},{13,9},{6,2},{10,6},{14,10},{7,3},{... | collective-permute-start | bytes 8456 | tf_op jit(solution)/shard_map/ppermute | solution.py:16
Sparse Core Ops, SparseCore 0:
  9.5 19.4 all-gather.4
  30.6 106.6 all-gather.6
  138.9 105.0 all-gather.8
  245.4 104.8 all-gather.10
  357.4 23.0 reduce-scatter.1
where the time goes:
time: 405 us
  waiting for transfers between devices  320 us (79%)
  blocking collectives  39.8 us (10%)
  matrix products  20.1 us (5%)
  between operations  13.9 us (3%)
  starting transfers between devices  9.15 us (2%)
    all_gather x1, waiting for transfers between devices, local(): lax.all_gather(down_weight, 'fs', axis=1, tiled=True)  108 us
    all_gather x1, waiting for transfers between devices, local(): lax.all_gather(up_weight, 'fs', axis=0, tiled=True)  100 us
    all_gather x1, waiting for transfers between devices, local(): lax.all_gather(gate_weight, 'fs', axis=0, tiled=True)  92.3 us
    psum x1, blocking collectives, local(): summed_conv = lax.psum(local_conv, ('rep', 'fs'))  34.5 us
    all_gather x1, waiting for transfers between devices, local(): grad_rows = lax.all_gather(out_grad, 'tp', axis=1, tiled=True)  8.16 us
  transfers between devices with their start and end apart: 9, of which 6 were waited for; matrix products, arithmetic and copies ran while one was open for 4% of the time, Pallas kernels for 0%

commit v1 on v0

--- a/solution.py
+++ b/solution.py
@@ -3,6 +3,23 @@
 import jax.numpy as jnp
 from jax import lax
 from jax.sharding import PartitionSpec as P
+
+
+def joined_along(tiles, dim):
+    lengths = list(tiles.shape[1:])
+    lengths[dim] *= tiles.shape[0]
+    return jnp.moveaxis(tiles, 0, dim).reshape(lengths)
+
+
+def ring_gather(x, axis, dim):
+    length = lax.axis_size(axis)
+    right = [(i, (i + 1) % length) for i in range(length)]
+    pieces = [x]
+    while len(pieces) < length:
+        pieces.append(lax.ppermute(pieces[-1], axis, right))
+    index = lax.axis_index(axis)
+    pieces = jnp.stack(pieces)[(index - jnp.arange(length)) % length]
+    return joined_along(pieces, dim)
 
 
 def extended(value, sides, width):
@@ -32,7 +49,7 @@
     grad_rows = lax.all_gather(out_grad, "tp", axis=1, tiled=True)
     act_grad = lax.dot_general(
         grad_rows,
-        lax.all_gather(down_weight, "fs", axis=1, tiled=True),
+        ring_gather(down_weight, "fs", 1),
         (((1,), (1,)), ((), ())),
         preferred_element_type=jnp.float32,
     )

time: 405 us -> 363 us (0.90)
  waiting for transfers between devices: 320 us -> 215 us
  starting transfers between devices: 9.15 us -> 48.5 us
  local copies, waits for them, and re-layouts: 0.74 us -> 17.5 us
  other arithmetic: 1.66 us -> 7.76 us
    all_gather x1 -> x0, waiting for transfers between devices: 108 us -> none  [local(): lax.all_gather(down_weight, 'fs', axis=1, tiled=True)]
    ppermute x0 -> x3, waiting for transfers between devices: none -> 104 us  [ring_gather(): pieces.append(lax.ppermute(pieces[-1], axis, right))]
    all_gather x1, waiting for transfers between devices: 92.3 us -> 0.02 us  [local(): lax.all_gather(gate_weight, 'fs', axis=0, tiled=True)]
    ppermute x2, waiting for transfers between devices: 0.03 us -> 39.3 us  [extended(): before = lax.ppermute(last, axis, up)]
    ppermute x0 -> x3, starting transfers between devices: none -> 38.1 us  [ring_gather(): pieces.append(lax.ppermute(pieces[-1], axis, right))]
    all_gather x1, waiting for transfers between devices: 100 us -> 63.7 us  [local(): lax.all_gather(up_weight, 'fs', axis=0, tiled=True)]
    transpose x0 -> x1, local copies, waits for them, and re-layouts: none -> 8.42 us  [joined_along(): return jnp.moveaxis(tiles, 0, dim).reshape(lengths)]
    all_gather x1, waiting for transfers between devices: 8.16 us -> 0.01 us  [local(): grad_rows = lax.all_gather(out_grad, 'tp', axis=1, tiled=True)]
  transfers between devices with their start and end apart: 9 -> 11, of which waited for: 6 -> 7; matrix products, arithmetic and copies ran while one was open for 4% -> 10% of each run, Pallas kernels for 0% -> 0%
where the time goes in v1:
time: 363 us
  waiting for transfers between devices  215 us (59%)
  starting transfers between devices  48.5 us (13%)
  blocking collectives  39.8 us (11%)
  matrix products  19.9 us (5%)
  local copies, waits for them, and re-layouts  17.5 us (5%)
  between operations  13.9 us (4%)
  other arithmetic  7.76 us (2%)
    ppermute x3, waiting for transfers between devices, ring_gather(): pieces.append(lax.ppermute(pieces[-1], axis, right))  104 us
    all_gather x1, waiting for transfers between devices, local(): lax.all_gather(up_weight, 'fs', axis=0, tiled=True)  63.7 us
    ppermute x2, waiting for transfers between devices, extended(): before = lax.ppermute(last, axis, up)  39.3 us
    ppermute x3, starting transfers between devices, ring_gather(): pieces.append(lax.ppermute(pieces[-1], axis, right))  38.1 us
    psum x1, blocking collectives, local(): summed_conv = lax.psum(local_conv, ('rep', 'fs'))  34.5 us
    transpose x1, local copies, waits for them, and re-layouts, joined_along(): return jnp.moveaxis(tiles, 0, dim).reshape(lengths)  8.42 us
    ppermute x2, starting transfers between devices, extended(): before = lax.ppermute(last, axis, up)  7.6 us
  transfers between devices with their start and end apart: 11, of which 7 were waited for; matrix products, arithmetic and copies ran while one was open for 10% of the time, Pallas kernels for 0%

profile of v1, /device:TPU:0, one launch (start us, length us, event | category | flops | bytes accessed | tf_op | source)
XLA Modules:
  0.0 362.5 jit_solution(1436198434852577471)
XLA Ops:
  7.2 0.0 all-gather.4.cloned.1.call-start
  7.2 0.7 all-gather.4.cloned.1.call-update
  7.9 0.0 copy-start
  7.9 0.0 all-gather.6.cloned.1.call-start
  8.0 0.7 all-gather.6.cloned.1.call-update
  8.7 0.0 all-gather.8.cloned.1.call-start
  8.7 0.7 all-gather.8.cloned.1.call-update
  9.4 0.0 reduce-scatter.2.cloned.1.call-start
  9.4 0.0 copy-done
  9.4 3.1 collective-permute-start
  12.6 36.9 %collective-permute-done = bf16[1408,512]{1,0:T(8,128)(2,1)S(1)} collective-permute-done((bf16[1408,512]{1,0:T(8,128)(2,1)S(1)}, bf16[1408,512]{1,0:T(8,128)(2,1)S(1)}, u32[]{:S(2)}, u32[]{:S(2)}) %collective-permute-start) | collective-permute-done | bytes 1441824 | tf_op jit(solution)/shard_map/ppermute | solution.py:19
  49.4 0.0 copy-start.1
  49.4 1.1 copy-done.1
  50.6 3.4 collective-permute-start.1
  53.9 65.4 %collective-permute-done.1 = bf16[1408,512]{1,0:T(8,128)(2,1)} collective-permute-done((bf16[1408,512]{1,0:T(8,128)(2,1)S(1)}, bf16[1408,512]{1,0:T(8,128)(2,1)}, u32[]{:S(2)}, u32[]{:S(2)}) %collective-permute-start.1) | collective-permute-done | bytes 1441824 | tf_op jit(solution)/shard_map/ppermute | solution.py:19
  119.3 31.7 %collective-permute-start.2 = (bf16[1408,512]{1,0:T(8,128)(2,1)}, bf16[1408,512]{1,0:T(8,128)(2,1)}, u32[]{:S(2)}, u32[]{:S(2)}) collective-permute-start(bf16[1408,512]{1,0:T(8,128)(2,1)} %collective-permute-done.1), channel_id=1, source_target_pairs={{0,4},{4,8},{8,12},{12,0},{1,5},{5,9},{9,13},{13,1},{2,6},{6,10},{... | collective-permute-start | bytes 4325384 | tf_op jit(solution)/shard_map/ppermute | solution.py:19
  151.0 0.8 fusion.18
  151.7 5.0 %collective-permute-start.3 = (bf16[1,1408]{1,0:T(2,128)(2,1)S(1)}, bf16[1,1408]{1,0:T(2,128)(2,1)S(1)}, u32[]{:S(2)}, u32[]{:S(2)}) collective-permute-start(bf16[1,1408]{1,0:T(2,128)(2,1)S(1)} %get-tuple-element.12), channel_id=1, source_target_pairs={{0,4},{4,8},{8,12},{1,5},{5,9},{9,13},{2,6},{6,10},{10,14},{3,7},{... | collective-permute-start | bytes 8456 | tf_op jit(solution)/shard_map/ppermute | solution.py:32
  156.7 1.3 collective-permute-start.4
  158.0 0.0 copy-start.2
  158.1 0.8 dynamic-slice_convert_fusion
  158.9 0.1 slice_reduce_fusion.2
  159.0 39.3 %collective-permute-done.3 = bf16[1,1408]{1,0:T(2,128)(2,1)S(1)} collective-permute-done((bf16[1,1408]{1,0:T(2,128)(2,1)S(1)}, bf16[1,1408]{1,0:T(2,128)(2,1)S(1)}, u32[]{:S(2)}, u32[]{:S(2)}) %collective-permute-start.3) | collective-permute-done | bytes 2848 | tf_op jit(solution)/shard_map/ppermute | solution.py:32
  198.2 0.0 collective-permute-done.4
  198.2 1.3 maximum_convert_fusion
  199.5 1.6 collective-permute-done.2
  201.1 0.0 copy-done.2
  201.1 4.9 %pad_maximum_fusion = bf16[4,1408,512]{2,1,0:T(8,128)(2,1)} fusion(bf16[1,1408,512]{2,1,0:T(8,128)(2,1)} %bitcast.3, bf16[1,1408,512]{2,1,0:T(8,128)(2,1)} %bitcast.2, bf16[1,1408,512]{2,1,0:T(8,128)(2,1)S(1)} %bitcast.17, bf16[1,1408,512]{2,1,0:T(8,128)(2,1)S(1)} %bitcast.16), kind=kLoop, calls=%fused_computation.1 | loop fusion | flops 8650752 | bytes 11534336 | tf_op jit(solution)/shard_map/stack | solution.py:21
  205.9 6.4 %gather_fusion = bf16[4,1408,512]{2,1,0:T(8,128)(2,1)} fusion(bf16[4,1408,512]{2,1,0:T(8,128)(2,1)} %pad_maximum_fusion, s32[1024]{0:T(1024)S(1)} %pad_clamp_fusion), kind=kCustom, calls=%fused_computation | custom fusion | bytes 11534352 | tf_op jit(solution)/shard_map/gather | solution.py:21
  212.4 0.0 copy-start.3
  212.4 8.4 %copy.9 = bf16[1408,4,512]{0,2,1:T(8,128)(2,1)} copy(bf16[1408,4,512]{2,0,1:T(8,128)(2,1)} %bitcast.14) | data formatting | bytes 11534336 | tf_op jit(solution)/shard_map/transpose | solution.py:11
  220.8 0.0 all-gather.4.cloned.1.call-done
  220.8 0.0 copy-done.3
  220.8 7.0 %fusion.6 = (bf16[256,1408]{1,0:T(8,128)(2,1)S(1)}, f32[256,1408]{1,0:T(8,128)}, f32[256,1408]{1,0:T(8,128)}) fusion(bf16[256,1408]{1,0:T(8,128)(2,1)S(1)} %copy-done.3, f32[258,1408]{1,0:T(8,128)S(1)} %maximum_convert_fusion, f32[1408]{0:T(1024)S(1)} %get-tuple-element.7, f32[1408]{0:T(1024)S(1)} %get-tuple-element.6, f32[1408]{0:T(1024)S(1)} %get-tuple-element.5, ...), kind=kOutput, calls=%fused_computation.11 | convolution fusion | flops 1482522624 | bytes 15483392 | tf_op jit(solution)/shard_map/dot_general | solution.py:50
  227.8 2.6 collective-permute-start.5
  230.4 1.3 collective-permute-start.6
  231.7 0.1 collective-permute-done.5
  231.8 6.2 %collective-permute-done.6 = bf16[1,1408]{1,0:T(2,128)(2,1)S(1)} collective-permute-done((bf16[1,1408]{1,0:T(2,128)(2,1)S(1)}, bf16[1,1408]{1,0:T(2,128)(2,1)S(1)}, u32[]{:S(2)}, u32[]{:S(2)}) %collective-permute-start.6) | collective-permute-done | bytes 2848 | tf_op jit(solution)/shard_map/ppermute | solution.py:33
  238.0 0.2 maximum_convert_fusion.1
  238.2 0.0 all-gather.6.cloned.1.call-done
  238.2 6.0 %fusion.10 = f32[256,2048]{1,0:T(8,128)} fusion(bf16[2048,1408]{1,0:T(8,128)(2,1)} %all-gather.6.cloned.1.call-done, f32[258,1408]{1,0:T(8,128)S(1)} %maximum_convert_fusion.1, f32[1408]{0:T(1024)S(1)} %get-tuple-element.7, f32[1408]{0:T(1024)S(1)} %get-tuple-element.6, f32[1408]{0:T(1024)S(1)} %get-tuple-element.5), kind=kOutput, calls=%fused_computation.25 | convolution fusion | flops 1478557696 | bytes 12214272 | tf_op jit(solution)/shard_map/dot_general | solution.py:77
  244.2 63.7 %all-gather.8.cloned.1.call-done = bf16[2048,1408]{1,0:T(8,128)(2,1)} async-done(((bf16[512,1408]{1,0:T(8,128)(2,1)}), bf16[2048,1408]{1,0:T(8,128)(2,1)}) %all-gather.8.cloned.1.call-update) | async-done | bytes 5767184 | tf_op jit(solution)/shard_map/all_gather | solution.py:85
  307.9 6.9 %fusion = bf16[256,2048]{1,0:T(8,128)(2,1)} fusion(f32[256,2048]{1,0:T(8,128)} %fusion.10, bf16[2048,1408]{1,0:T(8,128)(2,1)} %all-gather.8.cloned.1.call-done, f32[256,1408]{1,0:T(8,128)} %get-tuple-element.14, f32[256,1408]{1,0:T(8,128)} %get-tuple-element.9), kind=kOutput, calls=%fused_computation.4 | convolution fusion | flops 1479606272 | bytes 11796480 | tf_op jit(solution)/shard_map/dot_general | solution.py:83
  314.8 0.0 reduce-scatter.2.cloned.1.call-update
  314.9 0.6 multiply_reduce_fusion.2
  315.5 34.5 %psum.7 = f32[3,1408]{1,0:T(4,128)S(1)} all-reduce(f32[3,1408]{1,0:T(4,128)S(1)} %pad_maximum_fusion.1), channel_id=1, replica_groups=mesh['rep'=2,'fs'=4,'tp'=4] {'rep','fs'}, use_global_device_ids=true, to_apply=%region_4.5 | all-reduce | flops 4224 | bytes 33792 | tf_op jit(solution)/shard_map/psum | solution.py:92
  350.1 5.3 %all_gather.15 = f32[3,5632]{1,0:T(4,128)S(1)} all-gather(f32[3,1408]{1,0:T(4,128)S(1)} %psum.7), channel_id=1, replica_groups=mesh['rep'=2,'fs'=4,'tp'=4] {'tp'}, dimensions={1}, use_global_device_ids=true | all-gather | bytes 84480 | tf_op jit(solution)/shard_map/all_gather | solution.py:93
  355.4 0.0 reduce-scatter.2.cloned.1.call-done
  355.4 0.6 copy.11
  (7 shorter events, 0.1 us)
Async XLA Ops:
  7.2 213.6 %all-gather.4.cloned.1.call-start = ((), (), s32[]{:S(2)}) async-start(), calls=%async_computation.1 | async-start | bytes 1310720 | tf_op jit(solution)/shard_map/all_gather | solution.py:49
  7.9 1.5 copy-start
  7.9 230.3 %all-gather.6.cloned.1.call-start = ((), (), s32[]{:S(2)}) async-start(), calls=%async_computation.2 | async-start | bytes 7208960 | tf_op jit(solution)/shard_map/all_gather | solution.py:79
  8.7 299.3 %all-gather.8.cloned.1.call-start = ((), (), s32[]{:S(2)}) async-start(), calls=%async_computation.3 | async-start | bytes 7208960 | tf_op jit(solution)/shard_map/all_gather | solution.py:85
  9.4 346.0 %reduce-scatter.2.cloned.1.call-start = ((), (), s32[]{:S(2)}) async-start(), calls=%async_computation.4 | async-start | bytes 1310720 | tf_op jit(solution)/shard_map/reduce_scatter | solution.py:89
  9.4 40.0 %collective-permute-start = (bf16[1408,512]{1,0:T(8,128)(2,1)S(1)}, bf16[1408,512]{1,0:T(8,128)(2,1)S(1)}, u32[]{:S(2)}, u32[]{:S(2)}) collective-permute-start(bf16[1408,512]{1,0:T(8,128)(2,1)S(1)} %copy-done), channel_id=1, source_target_pairs={{0,4},{4,8},{8,12},{12,0},{1,5},{5,9},{9,13},{13,1},{2,6},{6,10},{... | collective-permute-start | bytes 4325384 | tf_op jit(solution)/shard_map/ppermute | solution.py:19
  49.4 1.1 copy-start.1
  50.6 68.7 %collective-permute-start.1 = (bf16[1408,512]{1,0:T(8,128)(2,1)S(1)}, bf16[1408,512]{1,0:T(8,128)(2,1)}, u32[]{:S(2)}, u32[]{:S(2)}) collective-permute-start(bf16[1408,512]{1,0:T(8,128)(2,1)S(1)} %collective-permute-done), channel_id=1, source_target_pairs={{0,4},{4,8},{8,12},{12,0},{1,5},{5,9},{9,13},{13,1},{2,6},{6,10},{... | collective-permute-start | bytes 4325384 | tf_op jit(solution)/shard_map/ppermute | solution.py:19
  119.3 81.8 %collective-permute-start.2 = (bf16[1408,512]{1,0:T(8,128)(2,1)}, bf16[1408,512]{1,0:T(8,128)(2,1)}, u32[]{:S(2)}, u32[]{:S(2)}) collective-permute-start(bf16[1408,512]{1,0:T(8,128)(2,1)} %collective-permute-done.1), channel_id=1, source_target_pairs={{0,4},{4,8},{8,12},{12,0},{1,5},{5,9},{9,13},{13,1},{2,6},{6,10},{... | collective-permute-start | bytes 4325384 | tf_op jit(solution)/shard_map/ppermute | solution.py:19
  151.7 46.5 %collective-permute-start.3 = (bf16[1,1408]{1,0:T(2,128)(2,1)S(1)}, bf16[1,1408]{1,0:T(2,128)(2,1)S(1)}, u32[]{:S(2)}, u32[]{:S(2)}) collective-permute-start(bf16[1,1408]{1,0:T(2,128)(2,1)S(1)} %get-tuple-element.12), channel_id=1, source_target_pairs={{0,4},{4,8},{8,12},{1,5},{5,9},{9,13},{2,6},{6,10},{10,14},{3,7},{... | collective-permute-start | bytes 8456 | tf_op jit(solution)/shard_map/ppermute | solution.py:32
  156.7 41.5 %collective-permute-start.4 = (bf16[1,1408]{1,0:T(2,128)(2,1)S(1)}, bf16[1,1408]{1,0:T(2,128)(2,1)S(1)}, u32[]{:S(2)}, u32[]{:S(2)}) collective-permute-start(bf16[1,1408]{1,0:T(2,128)(2,1)S(1)} %get-tuple-element.13), channel_id=1, source_target_pairs={{4,0},{8,4},{12,8},{5,1},{9,5},{13,9},{6,2},{10,6},{14,10},{7,3},{... | collective-permute-start | bytes 8456 | tf_op jit(solution)/shard_map/ppermute | solution.py:33
  158.0 43.0 %copy-start.2 = (bf16[1408,512]{1,0:T(8,128)(2,1)S(1)}, bf16[1408,512]{1,0:T(8,128)(2,1)}, u32[]{:S(2)}) copy-start(bf16[1408,512]{1,0:T(8,128)(2,1)} %copy-done.1) | copy-start | bytes 4325380
  212.4 8.4 %copy-start.3 = (bf16[256,1408]{1,0:T(8,128)(2,1)S(1)}, bf16[256,1408]{1,0:T(8,128)(2,1)}, u32[]{:S(2)}) copy-start(bf16[256,1408]{1,0:T(8,128)(2,1)} %param.9) | copy-start | bytes 2162692
  227.8 4.0 %collective-permute-start.5 = (bf16[1,1408]{1,0:T(2,128)(2,1)S(1)}, bf16[1,1408]{1,0:T(2,128)(2,1)S(1)}, u32[]{:S(2)}, u32[]{:S(2)}) collective-permute-start(bf16[1,1408]{1,0:T(2,128)(2,1)S(1)} %get-tuple-element.10), channel_id=1, source_target_pairs={{0,4},{4,8},{8,12},{1,5},{5,9},{9,13},{2,6},{6,10},{10,14},{3,7},{... | collective-permute-start | bytes 8456 | tf_op jit(solution)/shard_map/ppermute | solution.py:32
  230.4 7.6 %collective-permute-start.6 = (bf16[1,1408]{1,0:T(2,128)(2,1)S(1)}, bf16[1,1408]{1,0:T(2,128)(2,1)S(1)}, u32[]{:S(2)}, u32[]{:S(2)}) collective-permute-start(bf16[1,1408]{1,0:T(2,128)(2,1)S(1)} %get-tuple-element.11), channel_id=1, source_target_pairs={{4,0},{8,4},{12,8},{5,1},{9,5},{13,9},{6,2},{10,6},{14,10},{7,3},{... | collective-permute-start | bytes 8456 | tf_op jit(solution)/shard_map/ppermute | solution.py:33
Sparse Core Ops, SparseCore 0:
  9.5 19.4 all-gather.3
  30.6 170.7 all-gather.5
  202.9 104.9 all-gather.7
  315.0 23.0 reduce-scatter.1
